TPU v7x, 256 devices: a whole 4x4x8 slice. The times are simulated.
256 devices in a mesh: tp: 32 (over z, y), dp: 8 (over x, core).
Axes of the slice: x: 4, y: 4, z: 8, core: 2. Of those that a mesh axis runs over, the one named last changes fastest.
Arguments:
- tokens: bfloat16 [192, 1024], P('tp', 'dp'), may hold values from -6 to 6
- lengths: int32 [192], P('dp'), may hold values from 1 to 8, 384 in all
- norm_gain: float32 [2, 1024], P(None, 'dp'), may hold values from 0.1 to 1.9
- w_gate: bfloat16 [2, 1024, 2048], P(None, 'dp', 'tp'), may hold values from -0.1875 to 0.1875
- w_value: bfloat16 [2, 1024, 2048], P(None, 'dp', 'tp'), may hold values from -0.1875 to 0.1875
- w_write: bfloat16 [2, 1024, 256], P(None, 'dp', 'tp'), may hold values from -0.1875 to 0.1875
- w_read: bfloat16 [2, 1024, 256], P(None, 'dp', 'tp'), may hold values from -0.1875 to 0.1875
- w_step: bfloat16 [2, 1024, 32], P(None, 'dp', 'tp'), may hold values from -0.1875 to 0.1875
- step_bias: float32 [2, 32], P(None, 'tp'), may hold values from -1 to 1
- decay_rate: float32 [2, 32], P(None, 'tp'), may hold values from 0.5 to 4
- skip_gain: float32 [2, 32], P(None, 'tp'), may hold values from 0.5 to 2
- conv_value_w: float32 [2, 4, 2048], P(None, None, 'tp'), may hold values from -3 to 3
- conv_write_w: float32 [2, 4, 256], P(None, None, 'tp'), may hold values from -3 to 3
- conv_read_w: float32 [2, 4, 256], P(None, None, 'tp'), may hold values from -3 to 3
- group_gain: float32 [2, 2048], P(None, 'tp'), may hold values from 0.1 to 1.9
- w_out: bfloat16 [2, 2048, 1024], P(None, 'tp', 'dp'), may hold values from -0.125 to 0.125
- state: float32 [2, 192, 32, 64, 128], P(None, 'dp', 'tp'), may hold values from -0.6 to 0.6
- hist_value: bfloat16 [2, 192, 3, 2048], P(None, 'dp', None, 'tp'), may hold values from -6 to 6
- hist_write: bfloat16 [2, 192, 3, 256], P(None, 'dp', None, 'tp'), may hold values from -6 to 6
- hist_read: bfloat16 [2, 192, 3, 256], P(None, 'dp', None, 'tp'), may hold values from -6 to 6
Outputs:
- mixed: float32 [192, 1024], P('tp', 'dp')
- new_state: float32 [2, 192, 32, 64, 128], P(None, 'dp', 'tp')
- new_hist_value: bfloat16 [2, 192, 3, 2048], P(None, 'dp', None, 'tp')
- new_hist_write: bfloat16 [2, 192, 3, 256], P(None, 'dp', None, 'tp')
- new_hist_read: bfloat16 [2, 192, 3, 256], P(None, 'dp', None, 'tp')
Inputs may be any that keep to these rules, and one draw needn't show every extreme that they name: `lengths`: each sequence holds between 1 and 8 tokens before this step, and some sequence holds exactly 8.
All inputs are finite; a program needn't handle non-finite values.
Results may differ from a plain program's by a relative error of at most 0.03.
Values may be sent and summed in bfloat16 or wider, within the bound.
A program may use at most 64 MiB of HBM per device.

v0:
```python
import functools

import jax
import jax.numpy as jnp
from jax import lax
from jax.sharding import Mesh
from jax.sharding import PartitionSpec as P

D = 1024
GROUPS = 2
TP = ("tp_0", "tp_1")


norm_eps = 1e-05


def whole_of(x, axes, dim):
    if not axes:
        return x
    nearer = lax.all_gather(x, axes[-1], axis=dim, tiled=True)
    return whole_of(nearer, axes[:-1], dim)


def joined_along(pieces, dim):
    dims = list(pieces.shape[1:])
    dims[dim] *= pieces.shape[0]
    return jnp.moveaxis(pieces, 0, dim).reshape(dims)


def gather_together(arrays, axis, dims):
    vector = jnp.concatenate([a.reshape(-1) for a in arrays])
    lines, at, gathered = lax.all_gather(vector, axis), 0, []
    for a, dim in zip(arrays, dims):
        pieces = lines[:, at : at + a.size].reshape(-1, *a.shape)
        gathered.append(joined_along(pieces, dim))
        at += a.size
    return tuple(gathered)


def over_axes(x, axes):
    return functools.reduce(lax.psum, axes, x)


def scatter_axes(x, axes, dim):
    for axis in axes:
        x = lax.psum_scatter(x, axis, scatter_dimension=dim, tiled=True)
    return x


def conv_update(history, current, conv_taps, live_mask):
    kept_hist = history.astype(jnp.float32) * live_mask[:, :, None]
    mixed_sum = (
        jnp.sum(kept_hist * conv_taps[None, :-1, :], axis=1)
        + current.astype(jnp.float32) * conv_taps[-1][None, :]
    )
    fresh_hist = jnp.concatenate(
        [kept_hist[:, 1:].astype(jnp.bfloat16), current[:, None, :]], axis=1
    )
    return (jax.nn.silu(mixed_sum), fresh_hist)


def local(
    tokens,
    lengths,
    norm_gain,
    w_gate,
    w_value,
    w_write,
    w_read,
    w_step,
    step_bias,
    decay_rate,
    skip_gain,
    conv_value_w,
    conv_write_w,
    conv_read_w,
    group_gain,
    w_out,
    state,
    hist_value,
    hist_write,
    hist_read,
):
    seq_here = state.shape[1]
    local_heads = state.shape[2]
    head_dim = state.shape[3]
    hist_len = hist_value.shape[2]
    all_heads = local_heads * lax.axis_size(TP)
    per_group = all_heads // GROUPS
    group_width = all_heads * head_dim // GROUPS
    heads_here = lax.axis_index(TP) * local_heads + jnp.arange(local_heads, dtype=jnp.int32)
    group_here = heads_here // per_group
    member = (group_here[:, None] == jnp.arange(GROUPS, dtype=jnp.int32)[None, :]).astype(
        jnp.float32
    )
    offsets = hist_len - jnp.arange(hist_len, dtype=jnp.int32)
    live_mask = (offsets[None, :] <= lengths[:, None]).astype(jnp.float32)
    gate_cols = w_gate.shape[2]
    value_cols = w_value.shape[2]
    write_cols = w_write.shape[2]
    read_cols = w_read.shape[2]
    gathered = whole_of(tokens, TP, 0).astype(jnp.float32)
    current = tokens
    states_out, values_out, writes_out, reads_out = ([], [], [], [])
    for layer_idx in range(2):
        row_squares = jnp.sum(gathered * gathered, axis=1)
        weights = jnp.concatenate(
            [
                w_gate[layer_idx],
                w_value[layer_idx],
                w_write[layer_idx],
                w_read[layer_idx],
                w_step[layer_idx],
            ],
            axis=1,
        )
        total_sq = lax.psum(row_squares, "dp")
        row_scale = lax.rsqrt(total_sq / D + norm_eps)
        normed = (gathered * row_scale[:, None] * norm_gain[layer_idx][None, :]).astype(
            jnp.bfloat16
        )

        def project():
            row_block = lax.slice_in_dim(normed, 0, seq_here * lax.axis_size("dp"), axis=0)
            return jnp.dot(row_block, weights, preferred_element_type=jnp.float32)

        mixed_in = lax.psum_scatter(project(), "dp", scatter_dimension=0, tiled=True)
        edge_one = gate_cols
        edge_two = edge_one + value_cols
        edge_three = edge_two + write_cols
        edge_four = edge_three + read_cols
        gate_part = mixed_in[:, :edge_one].astype(jnp.bfloat16)
        value_part = mixed_in[:, edge_one:edge_two].astype(jnp.bfloat16)
        write_part = mixed_in[:, edge_two:edge_three].astype(jnp.bfloat16)
        read_part = mixed_in[:, edge_three:edge_four].astype(jnp.bfloat16)
        step_raw = mixed_in[:, edge_four:]
        value_act, value_hist = conv_update(
            hist_value[layer_idx], value_part, conv_value_w[layer_idx], live_mask
        )
        write_act, write_hist = conv_update(
            hist_write[layer_idx], write_part, conv_write_w[layer_idx], live_mask
        )
        read_act, read_hist = conv_update(
            hist_read[layer_idx], read_part, conv_read_w[layer_idx], live_mask
        )
        write_all, read_all = gather_together((write_act, read_act), TP, (1, 1))
        write_heads = jnp.moveaxis(
            jnp.take(write_all.reshape(seq_here, -1, GROUPS), group_here, axis=2), 2, 1
        )
        read_heads = jnp.moveaxis(
            jnp.take(read_all.reshape(seq_here, -1, GROUPS), group_here, axis=2), 2, 1
        )
        step_size = jax.nn.softplus(step_raw + step_bias[layer_idx][None, :])
        decay_keep = jnp.exp(-decay_rate[layer_idx][None, :] * step_size)
        inputs = value_act.reshape(seq_here, local_heads, head_dim)
        updated = (
            decay_keep[:, :, None, None] * state[layer_idx]
            + (step_size[:, :, None] * inputs)[:, :, :, None] * write_heads[:, :, None, :]
        )
        readout = (
            jnp.einsum("shpn,shn->shp", updated, read_heads, precision=lax.Precision.DEFAULT)
            + skip_gain[layer_idx][None, :, None] * inputs
        )
        gated_out = readout * jax.nn.silu(gate_part.astype(jnp.float32)).reshape(
            seq_here, local_heads, head_dim
        )
        head_squares = jnp.sum(gated_out * gated_out, axis=2)
        group_squares = jnp.dot(head_squares, member, precision=lax.Precision.DEFAULT)
        group_total = over_axes(group_squares, TP)
        group_scale = lax.rsqrt(group_total / group_width + norm_eps)
        head_scale = jnp.take(group_scale, group_here, axis=1)
        scaled_out = (gated_out * head_scale[:, :, None]).reshape(seq_here, -1)
        mixer_out = (scaled_out * group_gain[layer_idx][None, :]).astype(jnp.bfloat16)
        proj_out = w_out[layer_idx]

        def emit_rows(shard_rows):
            return jnp.dot(shard_rows, proj_out, preferred_element_type=jnp.float32)

        partial_value = emit_rows(lax.all_gather(mixer_out, "dp", axis=0, tiled=True))
        if layer_idx == 0:
            rounded = lax.optimization_barrier(over_axes(partial_value, TP).astype(jnp.bfloat16))
            gathered = rounded.astype(jnp.float32)
        else:
            current = scatter_axes(partial_value, TP, 0)
        states_out.append(updated)
        values_out.append(value_hist)
        writes_out.append(write_hist)
        reads_out.append(read_hist)
    return (
        current,
        jnp.stack(states_out),
        jnp.stack(values_out),
        jnp.stack(writes_out),
        jnp.stack(reads_out),
    )


def solution(mesh):
    torus = Mesh(mesh.devices.reshape(8, 4, mesh.shape["dp"]), ("tp_0", "tp_1", "dp"))
    return jax.shard_map(
        local,
        mesh=torus,
        in_specs=(
            P(TP, "dp"),
            P("dp"),
            P(None, "dp"),
            P(None, "dp", TP),
            P(None, "dp", TP),
            P(None, "dp", TP),
            P(None, "dp", TP),
            P(None, "dp", TP),
            P(None, TP),
            P(None, TP),
            P(None, TP),
            P(None, None, TP),
            P(None, None, TP),
            P(None, None, TP),
            P(None, TP),
            P(None, TP, "dp"),
            P(None, "dp", TP, None, None),
            P(None, "dp", None, TP),
            P(None, "dp", None, TP),
            P(None, "dp", None, TP),
        ),
        out_specs=(
            P(TP, "dp"),
            P(None, "dp", TP, None, None),
            P(None, "dp", None, TP),
            P(None, "dp", None, TP),
            P(None, "dp", None, TP),
        ),
        check_vma=False,
    )
```

profile of v0, /device:TPU:2, one launch (start us, length us, event | category | flops | bytes accessed | tf_op | source)
XLA Modules:
  0.0 469.3 jit_solution(14598672917770624518)
XLA Ops:
  7.2 0.8 slice_bitcast_fusion.20
  8.0 12.5 %all-gather.2 = bf16[4,6,128]{2,1,0:T(8,128)(2,1)S(1)} all-gather(bf16[1,6,128]{2,1,0:T(8,128)(2,1)} %bitcast.209), channel_id=1, replica_groups=mesh['tp_0'=8,'tp_1'=4,'dp'=8] {'tp_1'}, dimensions={0}, use_global_device_ids=true | all-gather | bytes 7680 | tf_op jit(solution)/shard_map/all_gather | solution.py:20
  20.4 28.1 %all_gather.25 = bf16[192,128]{1,0:T(8,128)(2,1)S(1)} all-gather(bf16[24,128]{1,0:T(8,128)(2,1)S(1)} %reshape.410), channel_id=1, replica_groups=mesh['tp_0'=8,'tp_1'=4,'dp'=8] {'tp_0'}, dimensions={0}, use_global_device_ids=true | all-gather | bytes 55296 | tf_op jit(solution)/shard_map/all_gather | solution.py:20
  48.7 10.1 %psum.56 = f32[192]{0:T(256)S(1)} all-reduce(f32[192]{0:T(256)S(1)} %fusion.16), channel_id=1, replica_groups=mesh['tp_0'=8,'tp_1'=4,'dp'=8] {'dp'}, use_global_device_ids=true, to_apply=%region_1.2 | all-reduce | flops 192 | bytes 1536 | tf_op jit(solution)/shard_map/psum | solution.py:117
  58.8 0.7 constant_dynamic-update-slice_fusion.4
  59.6 0.7 constant_dynamic-update-slice_fusion.3
  60.3 0.7 constant_dynamic-update-slice_fusion.2
  61.0 0.7 constant_dynamic-update-slice_fusion.1
  61.7 0.7 constant_dynamic-update-slice_fusion
  62.5 0.9 fusion.24
  63.5 0.7 slice_bitcast_fusion.19
  64.2 0.7 slice_bitcast_fusion.11
  64.9 0.7 slice_bitcast_fusion.17
  65.6 0.7 slice_bitcast_fusion.9
  66.4 1.3 fusion.48
  67.7 1.3 fusion.49
  70.3 1.3 fusion.50
  71.6 0.7 compare_convert_fusion.1
  72.3 0.8 convert_multiply_fusion.7
  73.1 0.8 multiply_reduce_fusion
  74.1 0.8 convert_multiply_fusion.10
  75.0 1.3 dynamic-slice.20
  76.9 0.8 multiply_reduce_fusion.5
  77.7 0.8 slice_bitcast_fusion.16
  78.5 14.3 %reduce-scatter.10.cloned.1.call-done = f32[24,145]{1,0:T(8,128)} async-done(((f32[192,145]{1,0:T(8,128)}), f32[24,145]{1,0:T(8,128)}) %reduce-scatter.10.cloned.1.call-update) | async-done | bytes 13936
  92.7 0.8 copy.142
  94.1 49.9 %all-gather.3 = f32[32,1,384]{2,1,0:T(1,128)S(1)} all-gather(f32[1,1,384]{2,1,0:T(1,128)S(1)} %reshape.411), channel_id=2, replica_groups=mesh['tp_0'=8,'tp_1'=4,'dp'=8] {'tp_0','tp_1'}, dimensions={0}, use_global_device_ids=true | all-gather | bytes 50688 | tf_op jit(solution)/shard_map/all_gather | solution.py:32
  144.2 0.6 exponential_bitcast_fusion.1
  146.1 0.8 multiply_reduce_fusion.3
  147.0 16.0 %psum.57 = f32[24,2]{0,1:T(2,128)S(1)} all-reduce(f32[24,2]{0,1:T(2,128)S(1)} %broadcast_multiply_fusion.3), channel_id=1, replica_groups=mesh['tp_0'=8,'tp_1'=4,'dp'=8] {'tp_0'}, use_global_device_ids=true, to_apply=%region_7.9 | all-reduce | flops 48 | bytes 384 | tf_op jit(solution)/shard_map/psum | solution.py:41
  163.0 9.1 %psum.58 = f32[24,2]{0,1:T(2,128)S(1)} all-reduce(f32[24,2]{0,1:T(2,128)S(1)} %psum.57), channel_id=1, replica_groups=mesh['tp_0'=8,'tp_1'=4,'dp'=8] {'tp_1'}, use_global_device_ids=true, to_apply=%region_8.10 | all-reduce | flops 48 | bytes 384 | tf_op jit(solution)/shard_map/psum | solution.py:41
  172.2 13.0 %all_gather.28 = bf16[192,64]{1,0:T(8,128)(2,1)S(1)} all-gather(bf16[24,64]{1,0:T(8,128)(2,1)S(1)} %copy.115), channel_id=1, replica_groups=mesh['tp_0'=8,'tp_1'=4,'dp'=8] {'dp'}, dimensions={0}, use_global_device_ids=true | all-gather | bytes 27648 | tf_op jit(solution)/shard_map/all_gather | solution.py:179
  185.2 0.8 fusion.40
  186.2 71.3 %all-reduce.4.cloned.1.call-done = f32[192,128]{1,0:T(8,128)} async-done(((f32[192,128]{1,0:T(8,128)}), f32[192,128]{1,0:T(8,128)}) %all-reduce.4.cloned.1.call-update) | async-done | bytes 98320 | tf_op jit(solution)/shard_map/psum | solution.py:41
  257.5 18.4 %psum.60 = bf16[192,128]{1,0:T(8,128)(2,1)S(1)} all-reduce(f32[192,128]{1,0:T(8,128)} %all-reduce.4.cloned.1.call-done), channel_id=1, replica_groups=mesh['tp_0'=8,'tp_1'=4,'dp'=8] {'tp_1'}, use_global_device_ids=true, to_apply=%region_10.13 | all-reduce | flops 24576 | bytes 147456 | tf_op jit(solution)/shard_map/psum | solution.py:41
  276.0 10.0 %psum.61 = f32[192]{0:T(256)S(1)} all-reduce(f32[192]{0:T(256)S(1)} %fusion.19), channel_id=1, replica_groups=mesh['tp_0'=8,'tp_1'=4,'dp'=8] {'dp'}, use_global_device_ids=true, to_apply=%region_12.15 | all-reduce | flops 192 | bytes 1536 | tf_op jit(solution)/shard_map/psum | solution.py:117
  286.0 0.9 fusion.22
  287.0 27.8 %reduce-scatter.12.cloned.1.call-done = f32[24,145]{1,0:T(8,128)} async-done(((f32[192,145]{1,0:T(8,128)}), f32[24,145]{1,0:T(8,128)}) %reduce-scatter.12.cloned.1.call-update) | async-done | bytes 13936
  314.8 0.8 copy.144
  316.2 50.0 %all-gather.4 = f32[32,1,384]{2,1,0:T(1,128)S(1)} all-gather(f32[1,1,384]{2,1,0:T(1,128)S(1)} %reshape.413), channel_id=3, replica_groups=mesh['tp_0'=8,'tp_1'=4,'dp'=8] {'tp_0','tp_1'}, dimensions={0}, use_global_device_ids=true | all-gather | bytes 50688 | tf_op jit(solution)/shard_map/all_gather | solution.py:32
  368.9 0.8 multiply_reduce_fusion.2
  369.7 15.9 %psum.62 = f32[24,2]{0,1:T(2,128)S(1)} all-reduce(f32[24,2]{0,1:T(2,128)S(1)} %broadcast_multiply_fusion.2), channel_id=1, replica_groups=mesh['tp_0'=8,'tp_1'=4,'dp'=8] {'tp_0'}, use_global_device_ids=true, to_apply=%region_18.21 | all-reduce | flops 48 | bytes 384 | tf_op jit(solution)/shard_map/psum | solution.py:41
  385.7 9.1 %psum.63 = f32[24,2]{0,1:T(2,128)S(1)} all-reduce(f32[24,2]{0,1:T(2,128)S(1)} %psum.62), channel_id=1, replica_groups=mesh['tp_0'=8,'tp_1'=4,'dp'=8] {'tp_1'}, use_global_device_ids=true, to_apply=%region_19.22 | all-reduce | flops 48 | bytes 384 | tf_op jit(solution)/shard_map/psum | solution.py:41
  395.0 13.1 %all_gather.31 = bf16[192,64]{1,0:T(8,128)(2,1)S(1)} all-gather(bf16[24,64]{1,0:T(8,128)(2,1)S(1)} %copy.126), channel_id=1, replica_groups=mesh['tp_0'=8,'tp_1'=4,'dp'=8] {'dp'}, dimensions={0}, use_global_device_ids=true | all-gather | bytes 27648 | tf_op jit(solution)/shard_map/all_gather | solution.py:179
  408.0 0.8 fusion.38
  410.7 1.2 pad_maximum_fusion
  411.9 32.8 %reduce-scatter.14.cloned.1.call-done = f32[24,128]{1,0:T(8,128)} async-done(((f32[192,128]{1,0:T(8,128)}), f32[24,128]{1,0:T(8,128)}) %reduce-scatter.14.cloned.1.call-update) | async-done | bytes 12304
  444.7 17.5 %all-reduce.1 = f32[24,128]{1,0:T(8,128)S(1)} all-reduce(f32[24,128]{1,0:T(8,128)} %reduce-scatter.14.cloned.1.call-done), channel_id=7, replica_groups=mesh['tp_0'=8,'tp_1'=4,'dp'=8] {'tp_1'}, use_global_device_ids=true, to_apply=%region_21.24.clone | all-reduce | flops 3072 | bytes 24576
  (96 shorter events, 8.8 us)
Async XLA Ops:
  7.2 85.6 %reduce-scatter.10.cloned.1.call-start = ((), (), s32[]{:S(2)}) async-start(), calls=%async_computation.4 | async-start | bytes 221184
  48.6 97.0 %copy-start = (f32[2,24,1,64,128]{4,3,2,1,0:T(8,128)S(1)}, f32[2,24,1,64,128]{4,3,2,1,0:T(8,128)}, u32[]{:S(2)}) copy-start(f32[2,24,1,64,128]{4,3,2,1,0:T(8,128)} %param.40) | copy-start | bytes 4718596
  63.4 194.1 %all-reduce.4.cloned.1.call-start = ((), (), s32[]{:S(2)}) async-start(), calls=%async_computation.3 | async-start | bytes 196608 | tf_op jit(solution)/shard_map/psum | solution.py:41
  78.5 106.8 %copy-start.1 = (bf16[2,64,128]{2,1,0:T(8,128)(2,1)S(1)}, bf16[2,64,128]{2,1,0:T(8,128)(2,1)}, u32[]{:S(2)}) copy-start(bf16[2,64,128]{2,1,0:T(8,128)(2,1)} %param.39) | copy-start | bytes 98308
  186.0 128.8 %reduce-scatter.12.cloned.1.call-start = ((), (), s32[]{:S(2)}) async-start(), calls=%async_computation.5 | async-start | bytes 221184
  287.0 157.7 %reduce-scatter.14.cloned.1.call-start = ((), (), s32[]{:S(2)}) async-start(), calls=%async_computation.6 | async-start | bytes 110592
Sparse Core Ops, SparseCore 0:
  63.5 29.1 reduce-scatter.9
  186.2 71.2 all-reduce.3
  287.1 27.6 reduce-scatter.11
  408.9 35.7 reduce-scatter.13
where the time goes:
time: 471 us; the launch traced here: 469 us
  blocking collectives  273 us (58%)
  waiting for transfers between devices  146 us (31%)
  local copies, waits for them, and re-layouts  18.1 us (4%)
  between operations  16.1 us (3%)
  other arithmetic  11.9 us (3%)
    all_gather x2, blocking collectives, gather_together(): lines, at, gathered = (lax.all_gather(vector, axis), 0, [])  99.9 us
    unnamed x7, waiting for transfers between devices  74.9 us
    psum x1, waiting for transfers between devices, over_axes(): return functools.reduce(lax.psum, axes, x)  71.3 us
    psum x5, blocking collectives, over_axes(): return functools.reduce(lax.psum, axes, x)  68.5 us
    all_gather x2, blocking collectives, whole_of(): nearer = lax.all_gather(x, axes[-1], axis=dim, tiled=True)  40.6 us
    all_gather x2, blocking collectives, local(): lax.all_gather(mixer_out, 'dp', axis=0, tiled=True)  26.1 us
    psum x2, blocking collectives, local(): total_sq = lax.psum(row_squares, 'dp')  20.1 us
    unnamed x1, blocking collectives  17.5 us
  transfers between devices with their start and end apart: 4, of which 4 were waited for; matrix products, arithmetic and copies ran while one was open for 3% of the time, Pallas kernels for 0%

commit v1 on v0

v1 whole, which is shorter than its diff:
```python
import functools

import jax
import jax.numpy as jnp
from jax import lax
from jax.experimental import pallas as pl
from jax.experimental.pallas import tpu as pltpu
from jax.sharding import PartitionSpec as P

MESH = pl.DeviceIdType.MESH
F32 = jnp.float32
BF16 = jnp.bfloat16
EPS = 1e-05

T0, IN0, IN1, OUT0, OUT1, GAIN, WR0, RS0, AG0, WR1, RS1 = range(11)


def iota(shape, dim):
    return lax.broadcasted_iota(jnp.int32, shape, dim)


def silu(x):
    return x / (1.0 + jnp.exp(-x))


def as_column(row):
    n = row.shape[1]
    square = jnp.broadcast_to(row, (n, n))
    return jnp.sum(jnp.where(iota((n, n), 0) == iota((n, n), 1), square, 0.0), axis=1, keepdims=True)


def dot(a, b, ca, cb):
    return lax.dot_general(a, b, (((ca,), (cb,)), ((), ())), preferred_element_type=F32)


def kernel(
    tok, lengths, ngain, wg, wv, ww, wr, ws, sb, dr, sg, cv, cw, cr, gg, wo, state, hv, hw, hr,
    mixed, nstate, nhv, nhw, nhr,
    tile_x, xbuf, wst, wfull, wofull, gain, st, nst, sel_n, cbv, t3v, cbwr, t3wr, ggc, wrsend, wrbuf, keepb, rsend, rbuf,
    ssem, rsem, lsem,
):
    t = lax.axis_index("tp")
    d = lax.axis_index("dp")
    z, y = t >> 2, t & 3
    own = z == d

    def dev(td, dd):
        return {"tp": td, "dp": dd}

    def send(src, dst, ex, td, dd):
        pltpu.make_async_remote_copy(
            src_ref=src, dst_ref=dst, send_sem=ssem.at[ex], recv_sem=rsem.at[ex],
            device_id=dev(td, dd), device_id_type=MESH,
        ).start()

    def wait(ref, sem):
        pltpu.make_async_copy(ref, ref, sem).wait()

    def wait_31_or_32(ref, sem):
        @pl.when(own)
        def _():
            wait(ref.at[0:31], sem)

        @pl.when(jnp.logical_not(own))
        def _():
            wait(ref, sem)

    def far_first(i):
        q, p = i >> 2, i & 3
        dz = 4 + (1 - 2 * (q & 1)) * ((q + 1) >> 1)
        dy = 2 + (1 - 2 * (p & 1)) * ((p + 1) >> 1)
        return (((z + dz) & 7) << 2) + ((y + dy) & 3)

    bar = pltpu.get_barrier_semaphore()

    def greet_tp(i, c):
        pl.semaphore_signal(bar, inc=1, device_id=dev(far_first(i), d), device_id_type=MESH)
        return c

    def greet_dp(i, c):
        pl.semaphore_signal(bar, inc=1, device_id=dev(t, (d + i) & 7), device_id_type=MESH)
        return c

    def greet_across(i, c):
        dd, td = i >> 2, 4 * d + (i & 3)

        @pl.when(jnp.logical_not((dd == d) & (td == t)))
        def _():
            pl.semaphore_signal(bar, inc=1, device_id=dev(td, dd), device_id_type=MESH)

        return c

    lax.fori_loop(0, 32, greet_across, 0)
    lax.fori_loop(0, 31, greet_tp, 0)
    lax.fori_loop(1, 8, greet_dp, 0)

    load = [pltpu.make_async_copy(state.at[l], st.at[l], lsem.at[l]) for l in range(2)]
    for l in range(2):
        load[l].start()

    tile_x[...] = jnp.zeros((8, 128), BF16)
    tile_x[0:6, :] = tok[...]
    for l in range(2):
        wst[l, 0:64, :] = wv[l]
        wst[l, 64:128, :] = wg[l]
        tail = jnp.concatenate(
            [ww[l].astype(F32), wr[l].astype(F32), ws[0, l : l + 1, :].astype(F32), jnp.zeros((15, 128), F32)], axis=0
        )
        wst[l, 128:160, :] = tail.astype(BF16)
        wfull[l, :, pl.ds(pl.multiple_of(d * 128, 128), 128)] = wst[l]
        wofull[l, :, pl.ds(pl.multiple_of(d * 128, 128), 128)] = wo[l]
    gain[:, pl.ds(pl.multiple_of(d * 128, 128), 128)] = ngain[...]

    srow = iota((24, 32), 0)
    six = (srow >= 6).astype(jnp.int32) + (srow >= 12).astype(jnp.int32) + (srow >= 18).astype(jnp.int32)
    place = (srow + 2 * six == iota((24, 32), 1)).astype(F32)
    place_b = place.astype(BF16)
    len_row = lengths[...].astype(F32)
    len_pad = jnp.dot(jnp.broadcast_to(len_row, (8, 24)).astype(BF16), place_b, preferred_element_type=F32)[0:1]
    len_col = as_column(len_row)
    for l in range(2):
        base_v = jnp.zeros((64, 32), F32)
        base_wr = jnp.zeros((16, 32), F32)
        for k in range(3):
            live_pad = (len_pad >= float(3 - k)).astype(F32)
            base_v += as_column(cv[l, k : k + 1, :]) * (dot(hv[l, k], place_b, 0, 0) * live_pad)
            base_w = as_column(cw[l, k : k + 1, :]) * (dot(hw[l, k], place_b, 1, 0) * live_pad)
            base_r = as_column(cr[l, k : k + 1, :]) * (dot(hr[l, k], place_b, 1, 0) * live_pad)
            base_wr += jnp.concatenate([base_w, base_r], axis=0)
            if k > 0:
                live_row = (len_row >= float(3 - k)).astype(F32)
                live_col = (len_col >= float(3 - k)).astype(F32)
                nhv[l, k - 1] = (hv[l, k].astype(F32) * live_col).astype(BF16)
                nhw[l, k - 1] = (hw[l, k].astype(F32) * live_row).astype(BF16)
                nhr[l, k - 1] = (hr[l, k].astype(F32) * live_row).astype(BF16)
        cbv[l] = base_v
        cbwr[l] = base_wr
        t3v[l] = jnp.broadcast_to(as_column(cv[l, 3:4, :]), (64, 32))
        t3wr[l] = jnp.broadcast_to(
            jnp.concatenate([as_column(cw[l, 3:4, :]), as_column(cr[l, 3:4, :])], axis=0), (16, 32)
        )
        ggc[l] = jnp.broadcast_to(as_column(gg[l : l + 1, :]), (64, 32))
    group = (t >= 16).astype(jnp.int32)
    sel_row = iota((256, 128), 0)
    sel_n[...] = (((sel_row >> 1) == iota((256, 128), 1)) & ((sel_row & 1) == group)).astype(F32).astype(BF16)

    pl.semaphore_wait(bar, 70 - own.astype(jnp.int32))

    def tokens_out(i, c):
        td = far_first(i)

        @pl.when(jnp.logical_not(own & (td == t)))
        def _():
            send(tile_x, xbuf.at[0, 4 * d + y], T0, td, z)

        return c

    lax.fori_loop(0, 32, tokens_out, 0)

    @pl.when(own)
    def _():
        xbuf[0, 4 * d + y] = tile_x[...]

    def weights_out(i, c):
        dd = (d + i) & 7
        col = pl.ds(pl.multiple_of(d * 128, 128), 128)
        send(ngain, gain.at[:, col], GAIN, t, dd)
        send(wst.at[0], wfull.at[0, :, col], IN0, t, dd)
        return c

    def weights_later(i, c):
        dd = (d + i) & 7
        col = pl.ds(pl.multiple_of(d * 128, 128), 128)
        send(wo.at[0], wofull.at[0, :, col], OUT0, t, dd)
        send(wst.at[1], wfull.at[1, :, col], IN1, t, dd)
        send(wo.at[1], wofull.at[1, :, col], OUT1, t, dd)
        return c

    lax.fori_loop(1, 8, weights_out, 0)
    lax.fori_loop(1, 8, weights_later, 0)

    wait_31_or_32(xbuf.at[0], rsem.at[T0])

    wait(gain.at[:, 0:896], rsem.at[GAIN])

    lane = iota((64, 32), 1)
    sub8 = iota((8, 128), 0)
    lane8 = iota((8, 128), 1)
    store = []
    for l in range(2):
        xs = [xbuf[l, 4 * a : 4 * a + 4].astype(F32).reshape(32, 128) for a in range(8)]
        squares = xs[0] * xs[0]
        for a in range(1, 8):
            squares += xs[a] * xs[a]
        scale = lax.rsqrt(jnp.sum(squares, axis=1, keepdims=True) / 1024.0 + EPS)
        normed = jnp.concatenate(
            [(xs[a] * scale * gain[l : l + 1, 128 * a : 128 * a + 128]).astype(BF16) for a in range(8)], axis=1
        )
        wait(wfull.at[l, :, 0:896], rsem.at[IN0 if l == 0 else IN1])
        proj = dot(wfull[l], normed, 1, 1)
        wr_new = proj[128:144].astype(BF16)
        wr_act = silu(cbwr[l] + t3wr[l] * wr_new.astype(F32))
        wr_tile = jnp.concatenate([wr_act[0:8], wr_act[8:16], jnp.zeros((8, 64), F32)], axis=1).astype(BF16)
        wrsend[l] = wr_tile
        ex = WR0 if l == 0 else WR1

        def maps_out(i, c):
            send(wrsend.at[l], wrbuf.at[l, t], ex, far_first(i), d)
            return c

        lax.fori_loop(0, 31, maps_out, 0)
        wrbuf[l, t] = wr_tile

        value_new = proj[0:64].astype(BF16)
        u = silu(cbv[l] + t3v[l] * value_new.astype(F32))
        gate = silu(proj[64:128].astype(BF16).astype(F32))
        raw = proj[144:145] + sb[0:1, l : l + 1]
        step = jnp.maximum(raw, 0.0) + jnp.log1p(jnp.exp(-jnp.abs(raw)))
        keep = jnp.exp(-dr[0:1, l : l + 1] * step)
        keepb[...] = jnp.broadcast_to(as_column(keep), (32, 128))
        su = u * step
        nhv[l, 2] = dot(place_b, value_new, 1, 1).astype(BF16)
        wr_nat = dot(wr_new, place_b, 1, 1)
        nhw[l, 2] = wr_nat[0:8].astype(BF16)
        nhr[l, 2] = wr_nat[8:16].astype(BF16)
        load[l].wait()

        wait(wrbuf.at[l, 0:31], rsem.at[ex])
        maps = dot(wrbuf[l].reshape(256, 128), sel_n[...], 0, 0)
        w_map = maps[0:32].astype(BF16)
        r_map = maps[32:64].astype(BF16)

        readout = jnp.zeros((64, 32), F32)
        for s in range(24):
            p = s + 2 * (s // 6)
            outer = dot(jnp.where(lane == p, su, 0.0).astype(BF16), w_map, 1, 0)
            new = keepb[p : p + 1, :] * st[l, s] + outer
            nst[l, s] = new
            readout = jnp.where(lane == p, dot(new.astype(BF16), r_map, 1, 1), readout)
        out_copy = pltpu.make_async_copy(nst.at[l], nstate.at[l], lsem.at[2 + l])
        out_copy.start()
        store.append(out_copy)

        gated = (readout + sg[0:1, l : l + 1] * u) * gate
        sq = jnp.sum(gated * gated, axis=0, keepdims=True)
        sq_hi = sq.astype(BF16).astype(F32)
        sq_lo = sq - sq_hi
        pad = jnp.zeros((1, 96), F32)
        row_hi = jnp.concatenate([sq_hi, pad], axis=1)
        row_lo = jnp.concatenate([sq_lo, pad], axis=1)
        mixer = (gated * ggc[l]).astype(BF16)
        wait(wofull.at[l, :, 0:896], rsem.at[OUT0 if l == 0 else OUT1])
        part = dot(mixer, wofull[l], 0, 0)
        for a in range(8):
            for k in range(4):
                piece = part[8 * k : 8 * k + 8, 128 * a : 128 * a + 128]
                piece = jnp.where(sub8 == 6, row_hi, jnp.where(sub8 == 7, row_lo, piece))
                rsend[l, 4 * a + k] = piece.astype(BF16)

        if l == 0:

            def parts_out(i, c):
                td = far_first(i)
                send(rsend.at[0, td], rbuf.at[0, t], RS0, td, d)
                return c

            lax.fori_loop(0, 31, parts_out, 0)
            rbuf[0, t] = rsend[0, t]
            wait(rbuf.at[0, 0:31], rsem.at[RS0])
        else:

            def parts_across(i, c):
                dd, td = i >> 2, 4 * d + (i & 3)

                @pl.when(jnp.logical_not((dd == d) & (td == t)))
                def _():
                    send(rsend.at[1, i], rbuf.at[1, t], RS1, td, dd)

                return c

            lax.fori_loop(0, 32, parts_across, 0)

            @pl.when(own)
            def _():
                rbuf[1, t] = rsend[1, t]

            wait_31_or_32(rbuf.at[1], rsem.at[RS1])

        total = jnp.zeros((8, 128), F32)
        for g in range(2):
            acc = jnp.sum(rbuf[l, 16 * g : 16 * g + 16].astype(F32), axis=0)
            sq_row = acc[6:7] + acc[7:8]
            sq_col = jnp.sum(
                jnp.where(lane8 == sub8 + 8 * y, jnp.broadcast_to(sq_row, (8, 128)), 0.0), axis=1, keepdims=True
            )
            total += acc * lax.rsqrt(sq_col / 1024.0 + EPS)
        if l == 0:
            tile = jnp.where(sub8 < 6, total, 0.0).astype(BF16)
            rsend[0, t] = tile

            def hidden_out(i, c):
                send(rsend.at[0, t], xbuf.at[1, t], AG0, far_first(i), d)
                return c

            lax.fori_loop(0, 31, hidden_out, 0)
            xbuf[1, t] = tile
            wait(xbuf.at[1, 0:31], rsem.at[AG0])
        else:
            mixed[...] = total[0:6]

    wait_31_or_32(xbuf.at[0], ssem.at[T0])
    wait_31_or_32(rbuf.at[1], ssem.at[RS1])
    wait(gain.at[:, 0:896], ssem.at[GAIN])
    for l in range(2):
        wait(wfull.at[l, :, 0:896], ssem.at[IN0 if l == 0 else IN1])
        wait(wofull.at[l, :, 0:896], ssem.at[OUT0 if l == 0 else OUT1])
        wait(wrbuf.at[l, 0:31], ssem.at[WR0 if l == 0 else WR1])
    wait(rbuf.at[0, 0:31], ssem.at[RS0])
    wait(xbuf.at[1, 0:31], ssem.at[AG0])
    for out_copy in store:
        out_copy.wait()


def local(
    tokens, lengths, norm_gain, w_gate, w_value, w_write, w_read, w_step, step_bias, decay_rate, skip_gain,
    conv_value_w, conv_write_w, conv_read_w, group_gain, w_out, state, hist_value, hist_write, hist_read,
):
    def flip(w):
        return jnp.transpose(w, (0, 2, 1))

    args = (
        tokens, lengths.reshape(1, 24), norm_gain, flip(w_gate), flip(w_value), flip(w_write), flip(w_read),
        jnp.transpose(w_step, (2, 0, 1)), step_bias.T, decay_rate.T, skip_gain.T,
        conv_value_w, conv_write_w, conv_read_w, group_gain, w_out, state.reshape(2, 24, 64, 128),
        jnp.transpose(hist_value, (0, 2, 1, 3)), jnp.transpose(hist_write, (0, 2, 3, 1)),
        jnp.transpose(hist_read, (0, 2, 3, 1)),
    )
    vmem = pl.BlockSpec(memory_space=pltpu.VMEM)
    hbm = pl.BlockSpec(memory_space=pl.ANY)
    mixed, nstate, nhv, nhw, nhr = pl.pallas_call(
        kernel,
        out_shape=(
            jax.ShapeDtypeStruct((6, 128), F32),
            jax.ShapeDtypeStruct((2, 24, 64, 128), F32),
            jax.ShapeDtypeStruct((2, 3, 24, 64), BF16),
            jax.ShapeDtypeStruct((2, 3, 8, 24), BF16),
            jax.ShapeDtypeStruct((2, 3, 8, 24), BF16),
        ),
        in_specs=[vmem] * 16 + [hbm] + [vmem] * 3,
        out_specs=(vmem, hbm, vmem, vmem, vmem),
        scratch_shapes=[
            pltpu.VMEM((8, 128), BF16),
            pltpu.VMEM((2, 32, 8, 128), BF16),
            pltpu.VMEM((2, 160, 128), BF16),
            pltpu.VMEM((2, 160, 1024), BF16),
            pltpu.VMEM((2, 64, 1024), BF16),
            pltpu.VMEM((2, 1024), F32),
            pltpu.VMEM((2, 24, 64, 128), F32),
            pltpu.VMEM((2, 24, 64, 128), F32),
            pltpu.VMEM((256, 128), BF16),
            pltpu.VMEM((2, 64, 32), F32),
            pltpu.VMEM((2, 64, 32), F32),
            pltpu.VMEM((2, 16, 32), F32),
            pltpu.VMEM((2, 16, 32), F32),
            pltpu.VMEM((2, 64, 32), F32),
            pltpu.VMEM((2, 8, 128), BF16),
            pltpu.VMEM((2, 32, 8, 128), BF16),
            pltpu.VMEM((32, 128), F32),
            pltpu.VMEM((2, 32, 8, 128), BF16),
            pltpu.VMEM((2, 32, 8, 128), BF16),
                pltpu.SemaphoreType.DMA((11,)),
            pltpu.SemaphoreType.DMA((11,)),
            pltpu.SemaphoreType.DMA((4,)),
        ],
        compiler_params=pltpu.CompilerParams(collective_id=0, has_side_effects=True),
    )(*args)
    return (
        mixed,
        nstate.reshape(2, 24, 1, 64, 128),
        jnp.transpose(nhv, (0, 2, 1, 3)),
        jnp.transpose(nhw, (0, 3, 1, 2)),
        jnp.transpose(nhr, (0, 3, 1, 2)),
    )


def solution(mesh):
    return jax.shard_map(
        local,
        mesh=mesh,
        in_specs=(
            P("tp", "dp"),
            P("dp"),
            P(None, "dp"),
            P(None, "dp", "tp"),
            P(None, "dp", "tp"),
            P(None, "dp", "tp"),
            P(None, "dp", "tp"),
            P(None, "dp", "tp"),
            P(None, "tp"),
            P(None, "tp"),
            P(None, "tp"),
            P(None, None, "tp"),
            P(None, None, "tp"),
            P(None, None, "tp"),
            P(None, "tp"),
            P(None, "tp", "dp"),
            P(None, "dp", "tp", None, None),
            P(None, "dp", None, "tp"),
            P(None, "dp", None, "tp"),
            P(None, "dp", None, "tp"),
        ),
        out_specs=(
            P("tp", "dp"),
            P(None, "dp", "tp", None, None),
            P(None, "dp", None, "tp"),
            P(None, "dp", None, "tp"),
            P(None, "dp", None, "tp"),
        ),
        check_vma=False,
    )
```

time: 471 us -> 62.1 us (0.13)
  the two profiles are of different devices: /device:TPU:2 before, /device:TPU:7 now
where the time goes in v1:
time: 62.1 us; the launch traced here: 61.8 us
  Pallas kernels  55.4 us (89%)
  local copies, waits for them, and re-layouts  5.83 us (9%)
  between operations  0.65 us (1%)
    pallas_call x1, Pallas kernels, local(): pl.pallas_call(kernel, out_shape=(jax.ShapeDtypeStruct((6, 128), F32), ja...  55.4 us
    unnamed x11, local copies, waits for them, and re-layouts  5.83 us

profile of v1, /device:TPU:7, one launch (start us, length us, event | category | flops | bytes accessed | tf_op | source)
XLA Modules:
  0.0 61.8 jit_solution(3441554644617297243)
XLA Ops:
  0.6 55.4 %shard_map.227 = (f32[6,128]{1,0:T(8,128)}, f32[2,24,64,128]{3,2,1,0:T(8,128)}, bf16[2,3,24,64]{3,2,1,0:T(8,128)(2,1)}, bf16[2,3,8,24]{3,2,1,0:T(8,128)(2,1)}, bf16[2,3,8,24]{3,2,1,0:T(8,128)(2,1)}) custom-call(bf16[6,128]{1,0:T(8,128)(2,1)} %tok.1, s32[1,24]{1,0:T(1,128)} %bitcast.31, f32[2,128]{1,0:T(2,128)} %ngain.1, bf16[2,64,128]{2,1,0:T(8,128)(2,1)} %bitcast.23, ...), custom_call_target="tpu_custom_call" | custom-call | tf_op jit(solution)/shard_map/pallas_call | solution.py:340
  56.0 1.3 %copy.31 = f32[6,128]{1,0:T(8,128)} copy(f32[6,128]{1,0:T(8,128)} %get-tuple-element.25) | data formatting | bytes 6144
  57.3 0.0 copy-start
  57.3 0.0 copy-start.2
  57.3 0.0 copy-start.1
  57.3 2.7 %copy.32 = f32[2,24,1,64,128]{4,3,2,1,0:T(8,128)} copy(f32[2,24,1,64,128]{4,3,2,1,0:T(8,128)} %bitcast.20) | data formatting | bytes 3145728
  60.0 0.0 copy-done
  60.0 0.6 copy.33
  60.6 0.0 copy-done.2
  60.6 0.6 copy.34
  61.2 0.0 copy-done.1
  61.2 0.6 copy.35
Async XLA Ops:
  57.3 2.7 %copy-start = (bf16[2,3,24,64]{3,2,1,0:T(8,128)(2,1)S(1)}, bf16[2,3,24,64]{3,2,1,0:T(8,128)(2,1)}, u32[]{:S(2)}) copy-start(bf16[2,3,24,64]{3,2,1,0:T(8,128)(2,1)} %get-tuple-element.12) | copy-start | bytes 55300
  57.3 3.4 %copy-start.2 = (bf16[2,3,8,24]{3,2,1,0:T(8,128)(2,1)S(1)}, bf16[2,3,8,24]{3,2,1,0:T(8,128)(2,1)}, u32[]{:S(2)}) copy-start(bf16[2,3,8,24]{3,2,1,0:T(8,128)(2,1)} %get-tuple-element.13) | copy-start | bytes 6916
  57.3 4.0 %copy-start.1 = (bf16[2,3,8,24]{3,2,1,0:T(8,128)(2,1)S(1)}, bf16[2,3,8,24]{3,2,1,0:T(8,128)(2,1)}, u32[]{:S(2)}) copy-start(bf16[2,3,8,24]{3,2,1,0:T(8,128)(2,1)} %get-tuple-element.14) | copy-start | bytes 6916

commit v2 on v1

v2 whole, which is shorter than its diff:
```python
import functools

import jax
import jax.numpy as jnp
from jax import lax
from jax.experimental import pallas as pl
from jax.experimental.pallas import tpu as pltpu
from jax.sharding import PartitionSpec as P

MESH = pl.DeviceIdType.MESH
F32 = jnp.float32
BF16 = jnp.bfloat16
EPS = 1e-05

T0, GAIN, INW0, INW1, IN0, IN1, OUT0, OUT1, WR0, CB, WP, RS0, AG0, RS1 = range(14)
EXCHANGES = 14


def iota(shape, dim):
    return lax.broadcasted_iota(jnp.int32, shape, dim)


def silu(x):
    return x / (1.0 + jnp.exp(-x))


def as_column(row):
    n = row.shape[1]
    square = jnp.broadcast_to(row, (n, n))
    return jnp.sum(jnp.where(iota((n, n), 0) == iota((n, n), 1), square, 0.0), axis=1, keepdims=True)


def as_row(column):
    n = column.shape[0]
    square = jnp.broadcast_to(column, (n, n))
    return jnp.sum(jnp.where(iota((n, n), 0) == iota((n, n), 1), square, 0.0), axis=0, keepdims=True)


def dot(a, b, ca, cb):
    return lax.dot_general(a, b, (((ca,), (cb,)), ((), ())), preferred_element_type=F32)


def kernel(
    tok, lengths, ngain, wg, wv, ww, wr, ws, sb, dr, sg, cv, cw, cr, gg, wo, state, hv, hw, hr,
    mixed, nstate, nhv, nhw, nhr,
    tile_x, xbuf, wst, wfull, wofull, gain, st, stb, sel, cbv, t3v, cbwr, t3wr, ggc,
    wrsend, wrbuf, rsend, rbuf, agsend, agbuf, cbsend, cbbuf, wpsend, wpbuf, wperm, keepb,
    ssem, rsem, lsem,
):
    t = lax.axis_index("tp")
    d = lax.axis_index("dp")
    z, y = t >> 2, t & 3
    own = z == d
    col = pl.ds(pl.multiple_of(d * 128, 128), 128)

    def dev(td, dd):
        return {"tp": td, "dp": dd}

    def send(src, dst, ex, td, dd):
        pltpu.make_async_remote_copy(
            src_ref=src, dst_ref=dst, send_sem=ssem.at[ex], recv_sem=rsem.at[ex],
            device_id=dev(td, dd), device_id_type=MESH,
        ).start()

    def wait(ref, sem):
        pltpu.make_async_copy(ref, ref, sem).wait()

    def wait_31_or_32(part, ref, sem):
        @pl.when(own)
        def _():
            wait(part, sem)

        @pl.when(jnp.logical_not(own))
        def _():
            wait(ref, sem)

    def far_first(i):
        q, p = i >> 2, i & 3
        dz = 4 + (1 - 2 * (q & 1)) * ((q + 1) >> 1)
        dy = 2 + (1 - 2 * (p & 1)) * ((p + 1) >> 1)
        return (((z + dz) & 7) << 2) + ((y + dy) & 3)

    def to_tp(body):
        def step(i, c):
            body(far_first(i))
            return c

        lax.fori_loop(0, 31, step, 0)

    def to_dp(body):
        def step(i, c):
            body((d + i) & 7)
            return c

        lax.fori_loop(1, 8, step, 0)

    def to_across(body):
        def step(i, c):
            dd, td = i >> 2, 4 * d + (i & 3)

            @pl.when(jnp.logical_not((dd == d) & (td == t)))
            def _():
                body(i, td, dd)

            return c

        lax.fori_loop(0, 32, step, 0)

    bar = pltpu.get_barrier_semaphore()

    def greet(td, dd):
        pl.semaphore_signal(bar, inc=1, device_id=dev(td, dd), device_id_type=MESH)

    to_across(lambda i, td, dd: greet(td, dd))
    to_tp(lambda td: greet(td, d))
    to_dp(lambda dd: greet(t, dd))

    load = [pltpu.make_async_copy(state.at[l], st.at[l], lsem.at[l]) for l in range(2)]
    for l in range(2):
        load[l].start()
    tile_x[...] = jnp.zeros((8, 128), BF16)
    tile_x[0:6, :] = tok[...]
    for l in range(2):
        head = jnp.concatenate(
            [ww[l].astype(F32), wr[l].astype(F32), ws[0, l : l + 1, :].astype(F32), jnp.zeros((15, 128), F32)], axis=0
        )
        wst[l, 0:32, :] = head.astype(BF16)
        wst[l, 32:96, :] = wv[l]
        wst[l, 96:160, :] = wg[l]

    pl.semaphore_wait(bar, 70 - own.astype(jnp.int32))

    def tokens_out(i, c):
        td = far_first(i)

        @pl.when(jnp.logical_not(own & (td == t)))
        def _():
            send(tile_x, xbuf.at[4 * d + y], T0, td, z)

        return c

    lax.fori_loop(0, 32, tokens_out, 0)

    @pl.when(own)
    def _():
        xbuf[4 * d + y] = tile_x[...]

    def first_weights(dd):
        send(ngain, gain.at[:, col], GAIN, t, dd)
        send(wst.at[0, 0:32], wfull.at[0, 0:32, col], INW0, t, dd)
        send(wst.at[1, 0:32], wfull.at[1, 0:32, col], INW1, t, dd)

    to_dp(first_weights)
    to_dp(lambda dd: send(wst.at[0, 32:160], wfull.at[0, 32:160, col], IN0, t, dd))
    to_dp(lambda dd: send(wo.at[0], wofull.at[0, :, col], OUT0, t, dd))
    to_dp(lambda dd: send(wst.at[1, 32:160], wfull.at[1, 32:160, col], IN1, t, dd))
    to_dp(lambda dd: send(wo.at[1], wofull.at[1, :, col], OUT1, t, dd))

    for l in range(2):
        wfull[l, :, col] = wst[l]
        wofull[l, :, col] = wo[l]
    gain[:, col] = ngain[...]
    srow = iota((24, 32), 0)
    six = (srow >= 6).astype(jnp.int32) + (srow >= 12).astype(jnp.int32) + (srow >= 18).astype(jnp.int32)
    place_b = (srow + 2 * six == iota((24, 32), 1)).astype(F32).astype(BF16)
    len_row = lengths[...].astype(F32)
    len_pad = jnp.dot(jnp.broadcast_to(len_row, (8, 24)).astype(BF16), place_b, preferred_element_type=F32)[0:1]
    len_col = as_column(len_row)
    for l in range(2):
        base_v = jnp.zeros((64, 32), F32)
        base_wr = jnp.zeros((16, 32), F32)
        for k in range(3):
            live_pad = (len_pad >= float(3 - k)).astype(F32)
            base_v += as_column(cv[l, k : k + 1, :]) * (dot(hv[l, k], place_b, 0, 0) * live_pad)
            base_w = as_column(cw[l, k : k + 1, :]) * (dot(hw[l, k], place_b, 1, 0) * live_pad)
            base_r = as_column(cr[l, k : k + 1, :]) * (dot(hr[l, k], place_b, 1, 0) * live_pad)
            base_wr += jnp.concatenate([base_w, base_r], axis=0)
            if k > 0:
                live_row = (len_row >= float(3 - k)).astype(F32)
                live_col = (len_col >= float(3 - k)).astype(F32)
                nhv[l, k - 1] = (hv[l, k].astype(F32) * live_col).astype(BF16)
                nhw[l, k - 1] = (hw[l, k].astype(F32) * live_row).astype(BF16)
                nhr[l, k - 1] = (hr[l, k].astype(F32) * live_row).astype(BF16)
        cbv[l] = base_v
        t3v[l] = jnp.broadcast_to(as_column(cv[l, 3:4, :]), (64, 32))
        tap_w = jnp.broadcast_to(as_column(cw[l, 3:4, :]), (8, 32))
        tap_r = jnp.broadcast_to(as_column(cr[l, 3:4, :]), (8, 32))
        if l == 0:
            cbwr[...] = base_wr
            t3wr[...] = jnp.concatenate([tap_w, tap_r], axis=0)
        else:
            cbsend[...] = jnp.concatenate([base_wr[0:8], base_wr[8:16], tap_w, tap_r], axis=1)
        ggc[l] = jnp.broadcast_to(as_column(gg[l : l + 1, :]), (64, 32))
    group = (t >= 16).astype(jnp.int32)
    sel_row = iota((256, 128), 0)
    for g in range(2):
        sel[g] = (((sel_row >> 1) == iota((256, 128), 1)) & ((sel_row & 1) == g)).astype(F32).astype(BF16)
    for l in range(2):
        load[l].wait()
        for s in range(24):
            stb[l, 64 * s : 64 * s + 64, :] = st[l, s].astype(BF16)

    wait_31_or_32(xbuf.at[0:31], xbuf, rsem.at[T0])
    wait(gain.at[:, 0:896], rsem.at[GAIN])

    lane = iota((64, 32), 1)
    sub8 = iota((8, 128), 0)
    lane8 = iota((8, 128), 1)
    for l in range(2):
        source = [xbuf[4 * a : 4 * a + 4] if l == 0 else agbuf[4 * a : 4 * a + 4, 0] for a in range(8)]
        xs = [x.astype(F32).reshape(32, 128) for x in source]
        squares = xs[0] * xs[0]
        for a in range(1, 8):
            squares += xs[a] * xs[a]
        scale = lax.rsqrt(jnp.sum(squares, axis=1, keepdims=True) / 1024.0 + EPS)
        normed = jnp.concatenate(
            [(xs[a] * scale * gain[l : l + 1, 128 * a : 128 * a + 128]).astype(BF16) for a in range(8)], axis=1
        )
        if l == 0:
            wait(wfull.at[0, 0:32, 0:896], rsem.at[INW0])
            first = dot(wfull[0, 0:32, :], normed, 1, 1)
            wr_new = first[0:16].astype(BF16)
            wr_act = silu(cbwr[...] + t3wr[...] * wr_new.astype(F32))
            wr_tile = jnp.concatenate([wr_act[0:8], wr_act[8:16], jnp.zeros((8, 64), F32)], axis=1).astype(BF16)
            wrsend[...] = wr_tile
            to_tp(lambda td: send(wrsend, wrbuf.at[t], WR0, td, d))
            wrbuf[t] = wr_tile
            wait(wfull.at[1, 0:32, 0:896], rsem.at[INW1])
            map_rows = wfull[1, 0:16, :].astype(F32)
            wpsend[0] = map_rows[0:8].astype(BF16)
            wpsend[1] = map_rows[8:16].astype(BF16)

            def piece_rows(td):
                return wpsend.at[:, :, pl.ds(pl.multiple_of((td >> 2) * 128, 128), 128)]

            to_tp(lambda td: send(piece_rows(td), wpbuf.at[:, t], WP, td, d))
            for m in range(2):
                wpbuf[m, t] = wpsend[m, :, pl.ds(pl.multiple_of(z * 128, 128), 128)]
            wait(wfull.at[0, 32:160, 0:896], rsem.at[IN0])
            rest = dot(wfull[0, 32:160, :], normed, 1, 1)
        else:
            wait(wfull.at[1, 32:160, 0:896], rsem.at[IN1])
            first = dot(wfull[1], normed, 1, 1)
            wr_new = first[0:16].astype(BF16)
            rest = first[32:160]
            maps = []
            for m in range(2):
                raw_map = agbuf[0:4, 1 + m].astype(F32)
                for a in range(1, 8):
                    raw_map += agbuf[4 * a : 4 * a + 4, 1 + m].astype(F32)
                new_map = (raw_map.reshape(32, 128) * scale).astype(BF16).astype(F32)
                maps.append(silu(conv_maps[32 * m : 32 * m + 32] + conv_maps[64 + 32 * m : 96 + 32 * m] * new_map))
            w_map, r_map = maps

        value_new = rest[0:64].astype(BF16)
        u = silu(cbv[l] + t3v[l] * value_new.astype(F32))
        gate = silu(rest[64:128].astype(BF16).astype(F32))
        raw = first[16:17] + sb[0:1, l : l + 1]
        step = jnp.maximum(raw, 0.0) + jnp.log1p(jnp.exp(-jnp.abs(raw)))
        keep = jnp.exp(-dr[0:1, l : l + 1] * step)
        su = u * step
        if l == 0:
            wait(wrbuf.at[0:31], rsem.at[WR0])
            maps = dot(wrbuf[...].reshape(256, 128), sel[group], 0, 0)
            w_map, r_map = maps[0:32], maps[32:64]
        r_b = r_map.astype(BF16)
        stored = dot(stb[l], r_b, 1, 1)
        readout = jnp.zeros((64, 32), F32)
        for s in range(24):
            p = s + 2 * (s // 6)
            readout = jnp.where(lane == p, stored[64 * s : 64 * s + 64], readout)
        wr_dot = as_row(jnp.sum(w_map * r_map, axis=1, keepdims=True))
        gated = (keep * readout + su * wr_dot + sg[0:1, l : l + 1] * u) * gate
        sq = jnp.sum(gated * gated, axis=0, keepdims=True)
        sq_hi = sq.astype(BF16).astype(F32)
        sq_lo = sq - sq_hi
        pad = jnp.zeros((1, 96), F32)
        row_hi = jnp.concatenate([sq_hi, pad], axis=1)
        row_lo = jnp.concatenate([sq_lo, pad], axis=1)
        mixer = (gated * ggc[l]).astype(BF16)
        wait(wofull.at[l, :, 0:896], rsem.at[OUT0 if l == 0 else OUT1])
        part = dot(mixer, wofull[l], 0, 0)
        for a in range(8):
            for k in range(4):
                piece = part[8 * k : 8 * k + 8, 128 * a : 128 * a + 128]
                piece = jnp.where(sub8 == 6, row_hi, jnp.where(sub8 == 7, row_lo, piece))
                rsend[l, 4 * a + k] = piece.astype(BF16)
        if l == 0:
            to_tp(lambda td: send(rsend.at[0, td], rbuf.at[0, t], RS0, td, d))
            rbuf[0, t] = rsend[0, t]
            to_tp(lambda td: send(cbsend, cbbuf.at[t], CB, td, d))
            cbbuf[t] = cbsend[...]
        else:
            to_across(lambda i, td, dd: send(rsend.at[1, i], rbuf.at[1, t], RS1, td, dd))

            @pl.when(own)
            def _():
                rbuf[1, t] = rsend[1, t]

        w_b = w_map.astype(BF16)
        keepb[...] = jnp.broadcast_to(as_column(keep), (32, 128))
        for s in range(24):
            p = s + 2 * (s // 6)
            outer = dot(jnp.where(lane == p, su, 0.0).astype(BF16), w_b, 1, 0)
            nstate[l, s] = keepb[p : p + 1, :] * st[l, s] + outer
        nhv[l, 2] = dot(place_b, value_new, 1, 1).astype(BF16)
        wr_nat = dot(wr_new, place_b, 1, 1)
        nhw[l, 2] = wr_nat[0:8].astype(BF16)
        nhr[l, 2] = wr_nat[8:16].astype(BF16)
        if l == 0:
            wait(wpbuf.at[:, 0:31], rsem.at[WP])
            for m in range(2):
                rows = wpbuf[m].reshape(256, 128)
                for g in range(2):
                    wperm[g, 128 * m : 128 * m + 128, :] = dot(sel[g], rows, 0, 0).astype(BF16)
            wait(rbuf.at[0, 0:31], rsem.at[RS0])
        else:
            wait_31_or_32(rbuf.at[1, 0:31], rbuf.at[1], rsem.at[RS1])

        total = jnp.zeros((8, 128), F32)
        for g in range(2):
            acc = jnp.sum(rbuf[l, 16 * g : 16 * g + 16].astype(F32), axis=0)
            sq_row = acc[6:7] + acc[7:8]
            sq_col = jnp.sum(
                jnp.where(lane8 == sub8 + 8 * y, jnp.broadcast_to(sq_row, (8, 128)), 0.0), axis=1, keepdims=True
            )
            total += acc * lax.rsqrt(sq_col / 1024.0 + EPS)
        if l == 0:
            tile = jnp.where(sub8 < 6, total, 0.0).astype(BF16)
            scaled = (tile.astype(F32) * gain[1:2, pl.ds(pl.multiple_of(z * 128, 128), 128)]).astype(BF16)
            for g in range(2):
                partial_maps = dot(scaled, wperm[g], 1, 1).astype(BF16)
                agsend[g, 0] = tile
                agsend[g, 1] = partial_maps[:, 0:128]
                agsend[g, 2] = partial_maps[:, 128:256]
            to_tp(lambda td: send(agsend.at[td >> 4], agbuf.at[t], AG0, td, d))
            agbuf[t] = agsend[group]
            wait(cbbuf.at[0:31], rsem.at[CB])
            conv_maps = lax.dot_general(
                cbbuf[...].reshape(256, 128), sel[group].astype(F32), (((0,), (0,)), ((), ())),
                precision=lax.Precision.HIGHEST, preferred_element_type=F32,
            )
            wait(agbuf.at[0:31], rsem.at[AG0])
        else:
            mixed[...] = total[0:6]

    wait_31_or_32(xbuf.at[0:31], xbuf, ssem.at[T0])
    wait_31_or_32(rbuf.at[1, 0:31], rbuf.at[1], ssem.at[RS1])
    wait(wpbuf.at[:, 0:31], ssem.at[WP])
    wait(gain.at[:, 0:896], ssem.at[GAIN])
    wait(wfull.at[0, 0:32, 0:896], ssem.at[INW0])
    wait(wfull.at[1, 0:32, 0:896], ssem.at[INW1])
    wait(wfull.at[0, 32:160, 0:896], ssem.at[IN0])
    wait(wfull.at[1, 32:160, 0:896], ssem.at[IN1])
    wait(wofull.at[0, :, 0:896], ssem.at[OUT0])
    wait(wofull.at[1, :, 0:896], ssem.at[OUT1])
    wait(wrbuf.at[0:31], ssem.at[WR0])
    wait(cbbuf.at[0:31], ssem.at[CB])
    wait(rbuf.at[0, 0:31], ssem.at[RS0])
    wait(agbuf.at[0:31], ssem.at[AG0])


def finish(*refs):
    given, outs, sem = refs[:5], refs[5:10], refs[10]
    copies = [pltpu.make_async_copy(a, b, sem.at[i]) for i, (a, b) in enumerate(zip(given, outs))]
    for copy in copies:
        copy.start()
    for copy in copies:
        copy.wait()


def local(
    tokens, lengths, norm_gain, w_gate, w_value, w_write, w_read, w_step, step_bias, decay_rate, skip_gain,
    conv_value_w, conv_write_w, conv_read_w, group_gain, w_out, state, hist_value, hist_write, hist_read,
):
    def flip(w):
        return jnp.transpose(w, (0, 2, 1))

    state = state.reshape(2, 24, 64, 128)
    args = (
        tokens, lengths.reshape(1, 24), norm_gain, flip(w_gate), flip(w_value), flip(w_write), flip(w_read),
        jnp.transpose(w_step, (2, 0, 1)), step_bias.T, decay_rate.T, skip_gain.T,
        conv_value_w, conv_write_w, conv_read_w, group_gain, w_out, state,
        jnp.transpose(hist_value, (0, 2, 1, 3)), jnp.transpose(hist_write, (0, 2, 3, 1)),
        jnp.transpose(hist_read, (0, 2, 3, 1)),
    )
    vmem = pl.BlockSpec(memory_space=pltpu.VMEM)
    hbm = pl.BlockSpec(memory_space=pl.ANY)
    outs = (
        ((6, 128), F32), ((2, 24, 64, 128), F32), ((2, 3, 24, 64), BF16), ((2, 3, 8, 24), BF16), ((2, 3, 8, 24), BF16),
    )
    held = pl.pallas_call(
        kernel,
        out_shape=tuple(pltpu.VMEM(*o) for o in outs),
        in_specs=[vmem] * 16 + [hbm] + [vmem] * 3,
        out_specs=(vmem,) * 5,
        scratch_shapes=[
            pltpu.VMEM((8, 128), BF16),
            pltpu.VMEM((32, 8, 128), BF16),
            pltpu.VMEM((2, 160, 128), BF16),
            pltpu.VMEM((2, 160, 1024), BF16),
            pltpu.VMEM((2, 64, 1024), BF16),
            pltpu.VMEM((2, 1024), F32),
            pltpu.VMEM((2, 24, 64, 128), F32),
            pltpu.VMEM((2, 1536, 128), BF16),
            pltpu.VMEM((2, 256, 128), BF16),
            pltpu.VMEM((2, 64, 32), F32),
            pltpu.VMEM((2, 64, 32), F32),
            pltpu.VMEM((16, 32), F32),
            pltpu.VMEM((16, 32), F32),
            pltpu.VMEM((2, 64, 32), F32),
            pltpu.VMEM((8, 128), BF16),
            pltpu.VMEM((32, 8, 128), BF16),
            pltpu.VMEM((2, 32, 8, 128), BF16),
            pltpu.VMEM((2, 32, 8, 128), BF16),
            pltpu.VMEM((2, 3, 8, 128), BF16),
            pltpu.VMEM((32, 3, 8, 128), BF16),
            pltpu.VMEM((8, 128), F32),
            pltpu.VMEM((32, 8, 128), F32),
            pltpu.VMEM((2, 8, 1024), BF16),
            pltpu.VMEM((2, 32, 8, 128), BF16),
            pltpu.VMEM((2, 256, 128), BF16),
            pltpu.VMEM((32, 128), F32),
            pltpu.SemaphoreType.DMA((EXCHANGES,)),
            pltpu.SemaphoreType.DMA((EXCHANGES,)),
            pltpu.SemaphoreType.DMA((2,)),
        ],
        compiler_params=pltpu.CompilerParams(collective_id=0, has_side_effects=True),
    )(*args)
    mixed, nstate, nhv, nhw, nhr = pl.pallas_call(
        finish,
        out_shape=tuple(jax.ShapeDtypeStruct(*o) for o in outs),
        in_specs=[vmem] * 5,
        out_specs=(hbm,) * 5,
        scratch_shapes=[pltpu.SemaphoreType.DMA((5,))],
    )(*(pltpu.with_memory_space_constraint(h, pltpu.VMEM) for h in held))
    return (
        mixed,
        nstate.reshape(2, 24, 1, 64, 128),
        jnp.transpose(nhv, (0, 2, 1, 3)),
        jnp.transpose(nhw, (0, 3, 1, 2)),
        jnp.transpose(nhr, (0, 3, 1, 2)),
    )


def solution(mesh):
    return jax.shard_map(
        local,
        mesh=mesh,
        in_specs=(
            P("tp", "dp"),
            P("dp"),
            P(None, "dp"),
            P(None, "dp", "tp"),
            P(None, "dp", "tp"),
            P(None, "dp", "tp"),
            P(None, "dp", "tp"),
            P(None, "dp", "tp"),
            P(None, "tp"),
            P(None, "tp"),
            P(None, "tp"),
            P(None, None, "tp"),
            P(None, None, "tp"),
            P(None, None, "tp"),
            P(None, "tp"),
            P(None, "tp", "dp"),
            P(None, "dp", "tp", None, None),
            P(None, "dp", None, "tp"),
            P(None, "dp", None, "tp"),
            P(None, "dp", None, "tp"),
        ),
        out_specs=(
            P("tp", "dp"),
            P(None, "dp", "tp", None, None),
            P(None, "dp", None, "tp"),
            P(None, "dp", None, "tp"),
            P(None, "dp", None, "tp"),
        ),
        check_vma=False,
    )
```

time: 62.1 us -> 49.3 us (0.79)
  Pallas kernels: 55.4 us -> 48.5 us
  local copies, waits for them, and re-layouts: 5.83 us -> 0 us
    pallas_call x1 -> x2, Pallas kernels: 55.4 us -> 48.5 us  [the longest x1 47.3 us: local(): pl.pallas_call(kernel, out_shape=tuple((pltpu.VMEM(*o) for o in outs)), i...]
    unnamed x11 -> x0, local copies, waits for them, and re-layouts: 5.83 us -> none
where the time goes in v2:
time: 49.3 us; the launch traced here: 49.1 us
  Pallas kernels  48.5 us (98%)
  between operations  0.65 us (1%)
    pallas_call x1, Pallas kernels, local(): pl.pallas_call(kernel, out_shape=tuple((pltpu.VMEM(*o) for o in outs)), i...  47.3 us
    pallas_call x1, Pallas kernels, local(): pl.pallas_call(finish, out_shape=tuple((jax.ShapeDtypeStruct(*o) for o in...  1.2 us

profile of v2, /device:TPU:7, one launch (start us, length us, event | category | flops | bytes accessed | tf_op | source)
XLA Modules:
  0.0 49.1 jit_solution(17107183792589166264)
XLA Ops:
  0.6 47.3 %shard_map.227 = (f32[6,128]{1,0:T(8,128)S(1)}, f32[2,24,64,128]{3,2,1,0:T(8,128)S(1)}, bf16[2,3,24,64]{3,2,1,0:T(8,128)(2,1)S(1)}, bf16[2,3,8,24]{3,2,1,0:T(8,128)(2,1)S(1)}, bf16[2,3,8,24]{3,2,1,0:T(8,128)(2,1)S(1)}) custom-call(bf16[6,128]{1,0:T(8,128)(2,1)} %tok.1, s32[1,24]{1,0:T(1,128)} %bitcast.27, f32[2,128]{1,0:T(2,128)} %ngain.1, ...), custom_call_target="tpu_custom_call" | custom-call | tf_op jit(solution)/shard_map/pallas_call | solution.py:392
  47.9 1.2 %shard_map.228 = (f32[6,128]{1,0:T(8,128)}, f32[2,24,64,128]{3,2,1,0:T(8,128)}, bf16[2,3,24,64]{3,2,1,0:T(8,128)(2,1)}, bf16[2,3,8,24]{3,2,1,0:T(8,128)(2,1)}, bf16[2,3,8,24]{3,2,1,0:T(8,128)(2,1)}) custom-call(f32[6,128]{1,0:T(8,128)S(1)} %get-tuple-element.15.refs_0_, f32[2,24,64,128]{3,2,1,0:T(8,128)S(1)} %get-tuple-element.16.refs_1_, ...), custom_call_target="tpu_custom_call" | custom-call | tf_op jit(solution)/shard_map/pallas_call | solution.py:430

commit v3 on v2

--- a/solution.py
+++ b/solution.py
@@ -40,13 +40,15 @@
     return lax.dot_general(a, b, (((ca,), (cb,)), ((), ())), preferred_element_type=F32)
 
 
-def kernel(
-    tok, lengths, ngain, wg, wv, ww, wr, ws, sb, dr, sg, cv, cw, cr, gg, wo, state, hv, hw, hr,
-    mixed, nstate, nhv, nhw, nhr,
-    tile_x, xbuf, wst, wfull, wofull, gain, st, stb, sel, cbv, t3v, cbwr, t3wr, ggc,
-    wrsend, wrbuf, rsend, rbuf, agsend, agbuf, cbsend, cbbuf, wpsend, wpbuf, wperm, keepb,
-    ssem, rsem, lsem,
-):
+def kernel(*refs):
+    given, state, outs, held, rest = refs[:19], refs[19], refs[20:25], refs[25:44], refs[44:]
+    tok, lengths, ngain, wg, wv, ww, wr, ws, sb, dr, sg, cv, cw, cr, gg, wo, hv, hw, hr = held
+    mixed, nstate, nhv, nhw, nhr = outs
+    (
+        tile_x, xbuf, wst, wfull, wofull, gain, st, stb, sel, cbv, t3v, cbwr, t3wr, ggc,
+        wrsend, wrbuf, rsend, rbuf, agsend, agbuf, cbsend, cbbuf, wpsend, wpbuf, wperm, keepb,
+        ssem, rsem, lsem, gsem,
+    ) = rest
     t = lax.axis_index("tp")
     d = lax.axis_index("dp")
     z, y = t >> 2, t & 3
@@ -111,15 +113,41 @@
     def greet(td, dd):
         pl.semaphore_signal(bar, inc=1, device_id=dev(td, dd), device_id_type=MESH)
 
-    to_across(lambda i, td, dd: greet(td, dd))
-    to_tp(lambda td: greet(td, d))
-    to_dp(lambda dd: greet(t, dd))
-
+    for dd in range(8):
+        for j in range(4):
+            alone = jnp.logical_not(own & (d == dd) & (y == j))
+            pl.when(alone)(functools.partial(greet, 4 * d + j, dd))
+    for i in range(1, 8):
+        greet(t, (d + i) & 7)
+
+    fetch = [pltpu.make_async_copy(a, b, gsem.at[i]) for i, (a, b) in enumerate(zip(given, held))]
+    for copy in fetch:
+        copy.start()
     load = [pltpu.make_async_copy(state.at[l], st.at[l], lsem.at[l]) for l in range(2)]
     for l in range(2):
         load[l].start()
+    fetch[0].wait()
     tile_x[...] = jnp.zeros((8, 128), BF16)
     tile_x[0:6, :] = tok[...]
+    pl.semaphore_wait(bar, 39 - own.astype(jnp.int32))
+
+    def tokens_out(i, c):
+        td = far_first(i)
+
+        @pl.when(jnp.logical_not(own & (td == t)))
+        def _():
+            send(tile_x, xbuf.at[4 * d + y], T0, td, z)
+
+        return c
+
+    lax.fori_loop(0, 32, tokens_out, 0)
+
+    @pl.when(own)
+    def _():
+        xbuf[4 * d + y] = tile_x[...]
+
+    for copy in fetch[1:]:
+        copy.wait()
     for l in range(2):
         head = jnp.concatenate(
             [ww[l].astype(F32), wr[l].astype(F32), ws[0, l : l + 1, :].astype(F32), jnp.zeros((15, 128), F32)], axis=0
@@ -127,23 +155,6 @@
         wst[l, 0:32, :] = head.astype(BF16)
         wst[l, 32:96, :] = wv[l]
         wst[l, 96:160, :] = wg[l]
-
-    pl.semaphore_wait(bar, 70 - own.astype(jnp.int32))
-
-    def tokens_out(i, c):
-        td = far_first(i)
-
-        @pl.when(jnp.logical_not(own & (td == t)))
-        def _():
-            send(tile_x, xbuf.at[4 * d + y], T0, td, z)
-
-        return c
-
-    lax.fori_loop(0, 32, tokens_out, 0)
-
-    @pl.when(own)
-    def _():
-        xbuf[4 * d + y] = tile_x[...]
 
     def first_weights(dd):
         send(ngain, gain.at[:, col], GAIN, t, dd)
@@ -380,9 +391,9 @@
     args = (
         tokens, lengths.reshape(1, 24), norm_gain, flip(w_gate), flip(w_value), flip(w_write), flip(w_read),
         jnp.transpose(w_step, (2, 0, 1)), step_bias.T, decay_rate.T, skip_gain.T,
-        conv_value_w, conv_write_w, conv_read_w, group_gain, w_out, state,
+        conv_value_w, conv_write_w, conv_read_w, group_gain, w_out,
         jnp.transpose(hist_value, (0, 2, 1, 3)), jnp.transpose(hist_write, (0, 2, 3, 1)),
-        jnp.transpose(hist_read, (0, 2, 3, 1)),
+        jnp.transpose(hist_read, (0, 2, 3, 1)), state,
     )
     vmem = pl.BlockSpec(memory_space=pltpu.VMEM)
     hbm = pl.BlockSpec(memory_space=pl.ANY)
@@ -392,9 +403,10 @@
     held = pl.pallas_call(
         kernel,
         out_shape=tuple(pltpu.VMEM(*o) for o in outs),
-        in_specs=[vmem] * 16 + [hbm] + [vmem] * 3,
+        in_specs=[pl.BlockSpec(memory_space=pltpu.HBM)] * 20,
         out_specs=(vmem,) * 5,
         scratch_shapes=[
+            *[pltpu.VMEM(a.shape, a.dtype) for a in args[:19]],
             pltpu.VMEM((8, 128), BF16),
             pltpu.VMEM((32, 8, 128), BF16),
             pltpu.VMEM((2, 160, 128), BF16),
@@ -424,6 +436,7 @@
             pltpu.SemaphoreType.DMA((EXCHANGES,)),
             pltpu.SemaphoreType.DMA((EXCHANGES,)),
             pltpu.SemaphoreType.DMA((2,)),
+            pltpu.SemaphoreType.DMA((19,)),
         ],
         compiler_params=pltpu.CompilerParams(collective_id=0, has_side_effects=True),
     )(*args)

time: 49.3 us -> 47.9 us (0.972)
  Pallas kernels: 48.5 us -> 47.2 us
    pallas_call x1, Pallas kernels: 47.3 us -> 46 us  [local(): pl.pallas_call(kernel, out_shape=tuple((pltpu.VMEM(*o) for o in outs)), i...]
where the time goes in v3:
time: 47.9 us; the launch traced here: 47.8 us
  Pallas kernels  47.2 us (99%)
  between operations  0.65 us (1%)
    pallas_call x1, Pallas kernels, local(): pl.pallas_call(kernel, out_shape=tuple((pltpu.VMEM(*o) for o in outs)), i...  46 us
    pallas_call x1, Pallas kernels, local(): pl.pallas_call(finish, out_shape=tuple((jax.ShapeDtypeStruct(*o) for o in...  1.2 us

profile of v3, /device:TPU:7, one launch (start us, length us, event | category | flops | bytes accessed | tf_op | source)
XLA Modules:
  0.0 47.8 jit_solution(5478892483898766754)
XLA Ops:
  0.6 46.0 %shard_map.227 = (f32[6,128]{1,0:T(8,128)S(1)}, f32[2,24,64,128]{3,2,1,0:T(8,128)S(1)}, bf16[2,3,24,64]{3,2,1,0:T(8,128)(2,1)S(1)}, bf16[2,3,8,24]{3,2,1,0:T(8,128)(2,1)S(1)}, bf16[2,3,8,24]{3,2,1,0:T(8,128)(2,1)S(1)}) custom-call(bf16[6,128]{1,0:T(8,128)(2,1)} %refs_0_.1, s32[1,24]{1,0:T(1,128)} %bitcast.27, f32[2,128]{1,0:T(2,128)} %refs_2_.1, ...), custom_call_target="tpu_custom_call" | custom-call | tf_op jit(solution)/shard_map/pallas_call | solution.py:403
  46.6 1.2 %shard_map.228 = (f32[6,128]{1,0:T(8,128)}, f32[2,24,64,128]{3,2,1,0:T(8,128)}, bf16[2,3,24,64]{3,2,1,0:T(8,128)(2,1)}, bf16[2,3,8,24]{3,2,1,0:T(8,128)(2,1)}, bf16[2,3,8,24]{3,2,1,0:T(8,128)(2,1)}) custom-call(f32[6,128]{1,0:T(8,128)S(1)} %get-tuple-element.15.refs_0_, f32[2,24,64,128]{3,2,1,0:T(8,128)S(1)} %get-tuple-element.16.refs_1_, ...), custom_call_target="tpu_custom_call" | custom-call | tf_op jit(solution)/shard_map/pallas_call | solution.py:443

commit v4 on v3

--- a/solution.py
+++ b/solution.py
@@ -12,8 +12,8 @@
 BF16 = jnp.bfloat16
 EPS = 1e-05
 
-T0, GAIN, INW0, INW1, IN0, IN1, OUT0, OUT1, WR0, CB, WP, RS0, AG0, RS1 = range(14)
-EXCHANGES = 14
+T0, GAIN, INW0, INW1, IN0, IN1, OUT0, OUT1, WR0, CB, WP, RS0, AG0, PM0, RS1 = range(15)
+EXCHANGES = 15
 
 
 def iota(shape, dim):
@@ -254,6 +254,19 @@
             first = dot(wfull[1], normed, 1, 1)
             wr_new = first[0:16].astype(BF16)
             rest = first[32:160]
+        value_new = rest[0:64].astype(BF16)
+        u = silu(cbv[l] + t3v[l] * value_new.astype(F32))
+        gate = silu(rest[64:128].astype(BF16).astype(F32))
+        raw = first[16:17] + sb[0:1, l : l + 1]
+        step = jnp.maximum(raw, 0.0) + jnp.log1p(jnp.exp(-jnp.abs(raw)))
+        keep = jnp.exp(-dr[0:1, l : l + 1] * step)
+        su = u * step
+        if l == 0:
+            wait(wrbuf.at[0:31], rsem.at[WR0])
+            maps = dot(wrbuf[...].reshape(256, 128), sel[group], 0, 0)
+            w_map, r_map = maps[0:32], maps[32:64]
+        else:
+            wait(agbuf.at[0:31, 1:3], rsem.at[PM0])
             maps = []
             for m in range(2):
                 raw_map = agbuf[0:4, 1 + m].astype(F32)
@@ -262,18 +275,6 @@
                 new_map = (raw_map.reshape(32, 128) * scale).astype(BF16).astype(F32)
                 maps.append(silu(conv_maps[32 * m : 32 * m + 32] + conv_maps[64 + 32 * m : 96 + 32 * m] * new_map))
             w_map, r_map = maps
-
-        value_new = rest[0:64].astype(BF16)
-        u = silu(cbv[l] + t3v[l] * value_new.astype(F32))
-        gate = silu(rest[64:128].astype(BF16).astype(F32))
-        raw = first[16:17] + sb[0:1, l : l + 1]
-        step = jnp.maximum(raw, 0.0) + jnp.log1p(jnp.exp(-jnp.abs(raw)))
-        keep = jnp.exp(-dr[0:1, l : l + 1] * step)
-        su = u * step
-        if l == 0:
-            wait(wrbuf.at[0:31], rsem.at[WR0])
-            maps = dot(wrbuf[...].reshape(256, 128), sel[group], 0, 0)
-            w_map, r_map = maps[0:32], maps[32:64]
         r_b = r_map.astype(BF16)
         stored = dot(stb[l], r_b, 1, 1)
         readout = jnp.zeros((64, 32), F32)
@@ -338,20 +339,22 @@
             total += acc * lax.rsqrt(sq_col / 1024.0 + EPS)
         if l == 0:
             tile = jnp.where(sub8 < 6, total, 0.0).astype(BF16)
+            agsend[0, 0] = tile
+            to_tp(lambda td: send(agsend.at[0, 0], agbuf.at[t, 0], AG0, td, d))
             scaled = (tile.astype(F32) * gain[1:2, pl.ds(pl.multiple_of(z * 128, 128), 128)]).astype(BF16)
             for g in range(2):
                 partial_maps = dot(scaled, wperm[g], 1, 1).astype(BF16)
-                agsend[g, 0] = tile
                 agsend[g, 1] = partial_maps[:, 0:128]
                 agsend[g, 2] = partial_maps[:, 128:256]
-            to_tp(lambda td: send(agsend.at[td >> 4], agbuf.at[t], AG0, td, d))
-            agbuf[t] = agsend[group]
+            to_tp(lambda td: send(agsend.at[td >> 4, 1:3], agbuf.at[t, 1:3], PM0, td, d))
+            agbuf[t, 0] = tile
+            agbuf[t, 1:3] = agsend[group, 1:3]
             wait(cbbuf.at[0:31], rsem.at[CB])
             conv_maps = lax.dot_general(
                 cbbuf[...].reshape(256, 128), sel[group].astype(F32), (((0,), (0,)), ((), ())),
                 precision=lax.Precision.HIGHEST, preferred_element_type=F32,
             )
-            wait(agbuf.at[0:31], rsem.at[AG0])
+            wait(agbuf.at[0:31, 0], rsem.at[AG0])
         else:
             mixed[...] = total[0:6]
 
@@ -368,7 +371,8 @@
     wait(wrbuf.at[0:31], ssem.at[WR0])
     wait(cbbuf.at[0:31], ssem.at[CB])
     wait(rbuf.at[0, 0:31], ssem.at[RS0])
-    wait(agbuf.at[0:31], ssem.at[AG0])
+    wait(agbuf.at[0:31, 0], ssem.at[AG0])
+    wait(agbuf.at[0:31, 1:3], ssem.at[PM0])
 
 
 def finish(*refs):

time: 47.9 us -> 47.1 us (0.983)
  Pallas kernels: 47.2 us -> 46.4 us
    pallas_call x1, Pallas kernels: 46 us -> 45.2 us  [local(): pl.pallas_call(kernel, out_shape=tuple((pltpu.VMEM(*o) for o in outs)), i...]
where the time goes in v4:
time: 47.1 us; the launch traced here: 47 us
  Pallas kernels  46.4 us (99%)
  between operations  0.65 us (1%)
    pallas_call x1, Pallas kernels, local(): pl.pallas_call(kernel, out_shape=tuple((pltpu.VMEM(*o) for o in outs)), i...  45.2 us
    pallas_call x1, Pallas kernels, local(): pl.pallas_call(finish, out_shape=tuple((jax.ShapeDtypeStruct(*o) for o in...  1.2 us

profile of v4, /device:TPU:7, one launch (start us, length us, event | category | flops | bytes accessed | tf_op | source)
XLA Modules:
  0.0 47.0 jit_solution(8489585190498333475)
XLA Ops:
  0.6 45.2 %shard_map.227 = (f32[6,128]{1,0:T(8,128)S(1)}, f32[2,24,64,128]{3,2,1,0:T(8,128)S(1)}, bf16[2,3,24,64]{3,2,1,0:T(8,128)(2,1)S(1)}, bf16[2,3,8,24]{3,2,1,0:T(8,128)(2,1)S(1)}, bf16[2,3,8,24]{3,2,1,0:T(8,128)(2,1)S(1)}) custom-call(bf16[6,128]{1,0:T(8,128)(2,1)} %refs_0_.1, s32[1,24]{1,0:T(1,128)} %bitcast.27, f32[2,128]{1,0:T(2,128)} %refs_2_.1, ...), custom_call_target="tpu_custom_call" | custom-call | tf_op jit(solution)/shard_map/pallas_call | solution.py:407
  45.8 1.2 %shard_map.228 = (f32[6,128]{1,0:T(8,128)}, f32[2,24,64,128]{3,2,1,0:T(8,128)}, bf16[2,3,24,64]{3,2,1,0:T(8,128)(2,1)}, bf16[2,3,8,24]{3,2,1,0:T(8,128)(2,1)}, bf16[2,3,8,24]{3,2,1,0:T(8,128)(2,1)}) custom-call(f32[6,128]{1,0:T(8,128)S(1)} %get-tuple-element.15.refs_0_, f32[2,24,64,128]{3,2,1,0:T(8,128)S(1)} %get-tuple-element.16.refs_1_, ...), custom_call_target="tpu_custom_call" | custom-call | tf_op jit(solution)/shard_map/pallas_call | solution.py:447

commit v5 on v4

--- a/solution.py
+++ b/solution.py
@@ -303,7 +303,18 @@
             to_tp(lambda td: send(cbsend, cbbuf.at[t], CB, td, d))
             cbbuf[t] = cbsend[...]
         else:
-            to_across(lambda i, td, dd: send(rsend.at[1, i], rbuf.at[1, t], RS1, td, dd))
+
+            def parts(i, c):
+                dd, k = (d + 4 + 2 * (i & 3) + ((i >> 2) & 1)) & 7, (i >> 3) & 3
+                td = 4 * d + k
+
+                @pl.when(jnp.logical_not((dd == d) & (td == t)))
+                def _():
+                    send(rsend.at[1, 4 * dd + k], rbuf.at[1, t], RS1, td, dd)
+
+                return c
+
+            lax.fori_loop(0, 32, parts, 0)
 
             @pl.when(own)
             def _():

time: 47.1 us -> 46.5 us (0.987)
  the two profiles are of different devices: /device:TPU:7 before, /device:TPU:1 now
where the time goes in v5:
time: 46.5 us; the launch traced here: 46.4 us
  Pallas kernels  45.8 us (98%)
  between operations  0.65 us (1%)
    pallas_call x1, Pallas kernels, local(): pl.pallas_call(kernel, out_shape=tuple((pltpu.VMEM(*o) for o in outs)), i...  44.6 us
    pallas_call x1, Pallas kernels, local(): pl.pallas_call(finish, out_shape=tuple((jax.ShapeDtypeStruct(*o) for o in...  1.2 us

profile of v5, /device:TPU:1, one launch (start us, length us, event | category | flops | bytes accessed | tf_op | source)
XLA Modules:
  0.0 46.4 jit_solution(10252686706458942483)
XLA Ops:
  0.6 44.6 %shard_map.227 = (f32[6,128]{1,0:T(8,128)S(1)}, f32[2,24,64,128]{3,2,1,0:T(8,128)S(1)}, bf16[2,3,24,64]{3,2,1,0:T(8,128)(2,1)S(1)}, bf16[2,3,8,24]{3,2,1,0:T(8,128)(2,1)S(1)}, bf16[2,3,8,24]{3,2,1,0:T(8,128)(2,1)S(1)}) custom-call(bf16[6,128]{1,0:T(8,128)(2,1)} %refs_0_.1, s32[1,24]{1,0:T(1,128)} %bitcast.27, f32[2,128]{1,0:T(2,128)} %refs_2_.1, ...), custom_call_target="tpu_custom_call" | custom-call | tf_op jit(solution)/shard_map/pallas_call | solution.py:418
  45.2 1.2 %shard_map.228 = (f32[6,128]{1,0:T(8,128)}, f32[2,24,64,128]{3,2,1,0:T(8,128)}, bf16[2,3,24,64]{3,2,1,0:T(8,128)(2,1)}, bf16[2,3,8,24]{3,2,1,0:T(8,128)(2,1)}, bf16[2,3,8,24]{3,2,1,0:T(8,128)(2,1)}) custom-call(f32[6,128]{1,0:T(8,128)S(1)} %get-tuple-element.15.refs_0_, f32[2,24,64,128]{3,2,1,0:T(8,128)S(1)} %get-tuple-element.16.refs_1_, ...), custom_call_target="tpu_custom_call" | custom-call | tf_op jit(solution)/shard_map/pallas_call | solution.py:458
